TPU v7x, 512 devices: a 4x2x32 block of a 4x8x32 slice. The times are simulated.
512 devices in a mesh: grp: 2 (over y), sp: 32 (over z), tp: 8 (over x, core).
Axes of the slice: x: 4, y: 2, z: 32, core: 2. Of those that a mesh axis runs over, the one named last changes fastest.
The devices are a block of a 4x8x32 slice.
Arguments:
- queries: bfloat16 [32768, 1024], P(('grp', 'sp'), 'tp'), parts along dimension 0, may hold values from -120 to 120
- keys: bfloat16 [32768, 256], P(('grp', 'sp')), parts along dimension 0, may hold values from -6 to 6
- values: bfloat16 [32768, 256], P(('grp', 'sp')), parts along dimension 0, may hold values from -6 to 6
- sink: float32 [8], P('tp'), may hold values from 1 to 5
- resid: bfloat16 [32768, 2048], P(('grp', 'sp')), parts along dimension 0, may hold values from -100 to 100
- out_proj: bfloat16 [1024, 2048], P(None, 'tp'), may hold values from -1.5 to 1.5
- norm_gain: float32 [2048], replicated, may hold values from 0.1 to 1.9
- w_gate: bfloat16 [2048, 6144], P('sp', 'tp'), may hold values from -0.125 to 0.125
- w_up: bfloat16 [2048, 6144], P('sp', 'tp'), may hold values from -0.125 to 0.125
- conv_w: float32 [3, 6144], P(None, 'tp'), may hold values from -3 to 3
- conv_b: float32 [6144], P('tp'), may hold values from -3 to 3
- w_down: bfloat16 [6144, 2048], P('tp', 'sp'), may hold values from -0.3125 to 0.3125
Outputs:
- layer_out: bfloat16 [32768, 2048], P(('grp', 'sp'), 'tp'), parts along dimension 0
There are 2 independent parts, one for each index of `grp`. A program takes and returns all parts, laid end to end along the dimension named above; an argument that names none is the same for every part. Nothing has to cross between parts.
All inputs are finite; a program needn't handle non-finite values.
Results may differ from a plain program's by a relative error of at most 0.015.
Values may be sent and summed in bfloat16 or wider, within the bound.
A program may use at most 64 MiB of HBM per device.

v0:
```python
import jax
import jax.numpy as jnp
from jax import lax
from jax.sharding import PartitionSpec as P

H = 8
KVH = 2
HD = 128
WINDOW = 128
CONV = 3


def sent_together(arrays, axis, dim, along):
    ends, at = ([], 0)
    for a in arrays[:-1]:
        at += a.shape[along]
        ends.append(at)
    both = jnp.concatenate(arrays, axis=along)
    return tuple(jnp.split(lax.all_gather(both, axis, axis=dim, tiled=True), ends, axis=along))


def with_halo(cells, sides, width):
    for axis, dim in sides:
        count = lax.axis_size(axis)
        ends = count - 1
        head = lax.slice_in_dim(cells, 0, width, axis=dim)
        tail = lax.slice_in_dim(cells, cells.shape[dim] - width, cells.shape[dim], axis=dim)
        cells = jnp.concatenate(
            [
                lax.ppermute(tail, axis, [(i, (i + 1) % count) for i in range(ends)]),
                cells,
                lax.ppermute(head, axis, [((i + 1) % count, i) for i in range(ends)]),
            ],
            axis=dim,
        )
    return cells


def sent_to_all(x, axis):
    copies = jnp.broadcast_to(x, (lax.axis_size(axis), *x.shape))
    return lax.all_to_all(copies, axis, split_axis=0, concat_axis=0, tiled=True)


def joined_along(blocks, dim):
    blocks = jnp.moveaxis(blocks, 0, dim)
    dims = blocks.shape
    return blocks.reshape(*dims[:dim], dims[dim] * dims[dim + 1], *dims[dim + 2 :])


def gathered_copies(x, axis, dim):
    blocks = sent_to_all(x, axis)
    return joined_along(blocks, dim)


def cut_along(x, dim, length):
    dims = x.shape
    blocks = x.reshape(*dims[:dim], length, dims[dim] // length, *dims[dim + 1 :])
    return jnp.moveaxis(blocks, dim, 0)


def sent_and_summed(x, axis, dim):
    blocks = cut_along(x, dim, lax.axis_size(axis))
    arrived = lax.all_to_all(blocks, axis, split_axis=0, concat_axis=0, tiled=True)
    return arrived.astype(jnp.float32).sum(axis=0)


def shards(
    queries, keys, values, sink, resid, out_proj, norm_gain, w_gate, w_up, conv_w, conv_b, w_down
):
    tokens = queries.shape[0]
    width = resid.shape[1]
    heads_here = sink.shape[0]
    group = H // KVH
    scale = HD ** (-0.5)
    whole_gate, whole_up = sent_together((w_gate, w_up), "sp", 0, 1)
    whole_down = lax.all_gather(w_down, "sp", axis=1, tiled=True)
    first_head = lax.axis_index("tp") * heads_here
    kv_head = first_head // group
    own_keys = lax.dynamic_slice_in_dim(keys, kv_head * HD, HD, 1)
    own_values = lax.dynamic_slice_in_dim(values, kv_head * HD, HD, 1)
    extended = with_halo(jnp.stack([own_keys, own_values]), (("sp", 1),), WINDOW)
    ext_keys = extended[0]
    ext_values = extended[1]
    span = tokens + 2 * WINDOW
    q_heads = queries.reshape(tokens, heads_here, HD)
    scores = (
        jnp.einsum("qhd,kd->hqk", q_heads, ext_keys, preferred_element_type=jnp.float32) * scale
    )
    offset = lax.axis_index("sp") * tokens
    q_pos = offset + jnp.arange(tokens, dtype=jnp.int32)[:, None]
    k_pos = offset - WINDOW + jnp.arange(span, dtype=jnp.int32)[None, :]
    seq_total = tokens * lax.axis_size("sp")
    valid = (jnp.abs(q_pos - k_pos) <= WINDOW) & (k_pos >= 0) & (k_pos < seq_total)
    scores = jnp.where(valid[None], scores, jnp.float32(-1e30))
    sink_col = sink[:, None]
    top = jnp.maximum(jnp.max(scores, axis=-1), sink_col)
    expo = jnp.exp(scores - top[..., None])
    total = jnp.sum(expo, axis=-1) + jnp.exp(sink_col - top)
    weights = (expo / total[..., None]).astype(jnp.bfloat16)
    heads_out = jnp.einsum("hqk,kd->qhd", weights, ext_values, preferred_element_type=jnp.float32)
    heads_out = heads_out.astype(jnp.bfloat16).reshape(tokens, heads_here * HD)
    all_heads = gathered_copies(heads_out, "tp", 1)
    cols = width // lax.axis_size("tp")
    col_start = lax.axis_index("tp") * cols
    full_proj = gathered_copies(out_proj, "tp", 1)
    summed = resid.astype(jnp.float32) + jnp.dot(
        all_heads, full_proj, preferred_element_type=jnp.float32
    )
    mean = jnp.mean(summed, axis=-1, keepdims=True)
    msq = jnp.mean(summed * summed, axis=-1, keepdims=True)
    normed_full = ((summed - mean) * lax.rsqrt(msq - mean * mean + 1e-05) * norm_gain).astype(
        jnp.bfloat16
    )
    normed_own = lax.dynamic_slice_in_dim(normed_full, col_start, cols, 1)
    gate_acc = jnp.dot(normed_full, whole_gate, preferred_element_type=jnp.float32)
    up_acc = jnp.dot(normed_full, whole_up, preferred_element_type=jnp.float32)
    gate_pre = gate_acc.astype(jnp.bfloat16)
    up_part = up_acc.astype(jnp.bfloat16)
    padded = with_halo(gate_pre, (("sp", 0),), CONV // 2)
    conv = conv_b
    for tap in range(CONV):
        conv = conv + padded[tap : tap + tokens].astype(jnp.float32) * conv_w[tap]
    act = (jax.nn.silu(conv) * up_part.astype(jnp.float32)).astype(jnp.bfloat16)
    terms = jnp.dot(act, whole_down, preferred_element_type=jnp.float32)
    ffn_own = sent_and_summed(terms.astype(jnp.bfloat16), "tp", 1)
    return (normed_own.astype(jnp.float32) + ffn_own).astype(jnp.bfloat16)


def solution(mesh):
    return jax.shard_map(
        shards,
        mesh=mesh,
        in_specs=(
            P(("grp", "sp"), "tp"),
            P(("grp", "sp"), None),
            P(("grp", "sp"), None),
            P("tp"),
            P(("grp", "sp"), None),
            P(None, "tp"),
            P(),
            P("sp", "tp"),
            P("sp", "tp"),
            P(None, "tp"),
            P("tp"),
            P("tp", "sp"),
        ),
        out_specs=P(("grp", "sp"), "tp"),
        check_vma=False,
    )
```

profile of v0, /device:TPU:33, one launch (start us, length us, event | category | flops | bytes accessed | tf_op | source)
XLA Modules:
  0.0 364.9 jit_solution(8369022057963651596)
XLA Ops:
  6.6 1.7 pad_maximum_fusion.5
  8.3 1.0 dynamic-slice_bitcast_fusion
  9.3 5.3 %collective-permute-start = (bf16[2,128,128]{2,1,0:T(8,128)(2,1)S(1)}, bf16[2,128,128]{2,1,0:T(8,128)(2,1)S(1)}, u32[]{:S(2)}, u32[]{:S(2)}) collective-permute-start(bf16[2,128,128]{2,1,0:T(8,128)(2,1)S(1)} %get-tuple-element.12), channel_id=1, source_target_pairs={{0,8},{8,16},{16,24},{24,32},{32,40},{40,48},{48,56},{56,64},{64,7... | collective-permute-start | bytes 196616 | tf_op jit(solution)/shard_map/ppermute | solution.py:30
  14.6 1.3 collective-permute-start.1
  16.6 4.1 %collective-permute-done.1 = bf16[2,128,128]{2,1,0:T(8,128)(2,1)S(1)} collective-permute-done((bf16[2,128,128]{2,1,0:T(8,128)(2,1)S(1)}, bf16[2,128,128]{2,1,0:T(8,128)(2,1)S(1)}, u32[]{:S(2)}, u32[]{:S(2)}) %collective-permute-start.1) | collective-permute-done | bytes 65568 | tf_op jit(solution)/shard_map/ppermute | solution.py:32
  20.7 0.8 fusion.32
  22.2 1.1 broadcast_in_dim.9
  23.3 41.1 %all-to-all-start = ((bf16[8,512,128]{1,2,0:T(8,128)(2,1)}), bf16[8,512,128]{1,2,0:T(8,128)(2,1)S(1)}, u32[]{:S(2)}, u32[]{:S(2)}) async-start(bf16[8,512,128]{1,2,0:T(8,128)(2,1)} %broadcast_in_dim.9), calls=%async_computation | async-start | bytes 2097152 | tf_op jit(solution)/shard_map/all_to_all | solution.py:41
  64.3 0.8 all-gather.5.cloned.1.call-update
  65.3 14.1 %all-to-all-done = bf16[8,512,128]{1,2,0:T(8,128)(2,1)S(1)} async-done(((bf16[8,512,128]{1,2,0:T(8,128)(2,1)}), bf16[8,512,128]{1,2,0:T(8,128)(2,1)S(1)}, u32[]{:S(2)}, u32[]{:S(2)}) %all-to-all-start) | async-done | bytes 1048608 | tf_op jit(solution)/shard_map/all_to_all | solution.py:41
  79.4 0.5 broadcast_in_dim.10
  79.9 52.3 %all_to_all.15 = bf16[8,1024,256]{1,2,0:T(8,128)(2,1)S(1)} all-to-all(bf16[8,1024,256]{1,2,0:T(8,128)(2,1)S(1)} %broadcast_in_dim.10), channel_id=1, replica_groups=mesh['grp'=2,'sp'=32,'tp'=8] {'tp'}, dimensions={0} | all-to-all | bytes 8388608 | tf_op jit(solution)/shard_map/all_to_all | solution.py:41
  132.2 2.9 fusion.30
  135.2 0.6 multiply_convert_fusion
  135.9 26.1 %all-gather.3.cloned.1.call-done = bf16[2048,1536]{1,0:T(8,128)(2,1)} async-done(((bf16[64,1536]{1,0:T(8,128)(2,1)}), bf16[2048,1536]{1,0:T(8,128)(2,1)}) %all-gather.3.cloned.1.call-update) | async-done | bytes 6291472 | tf_op jit(solution)/shard_map/all_gather | solution.py:19
  162.0 3.7 %fusion.6 = bf16[512,768]{1,0:T(8,128)(2,1)S(1)} fusion(bf16[512,2048]{1,0:T(8,128)(2,1)S(1)} %multiply_convert_fusion, bf16[2048,1536]{1,0:T(8,128)(2,1)} %all-gather.3.cloned.1.call-done), kind=kOutput, calls=%fused_computation.17 | convolution fusion | flops 1611005952 | bytes 6029312 | tf_op jit(solution)/shard_map/dot_general | solution.py:115
  165.7 2.8 collective-permute-start.2
  168.4 1.3 collective-permute-start.3
  169.8 123.4 %all-gather.5.cloned.1.call-done = bf16[768,2048]{0,1:T(8,128)(2,1)} async-done(((bf16[768,64]{0,1:T(8,128)(2,1)}), bf16[768,2048]{0,1:T(8,128)(2,1)}) %all-gather.5.cloned.1.call-update) | async-done | bytes 3145744 | tf_op jit(solution)/shard_map/all_gather | solution.py:76
  293.2 8.4 %convolution_convert_fusion = bf16[512,2048]{1,0:T(8,128)(2,1)} fusion(bf16[768,2048]{0,1:T(8,128)(2,1)} %all-gather.5.cloned.1.call-done, bf16[512,768]{1,0:T(8,128)(2,1)S(1)} %fusion.6, bf16[512,2048]{1,0:T(8,128)(2,1)S(1)} %multiply_convert_fusion, bf16[2048,1536]{1,0:T(8,128)(2,1)} %all-gather.3.cloned.1.call-done, ...), kind=kOutput, calls=%fused_computation.8 | convolution fusion | flops 3231318016 | bytes 11287552 | tf_op jit(solution)/shard_map/dot_general | solution.py:124
  301.6 3.1 copy.19
  304.7 25.2 %all-to-all-start.2 = ((bf16[8,512,256]{2,1,0:T(8,128)(2,1)}), bf16[8,512,256]{2,1,0:T(8,128)(2,1)S(1)}, u32[]{:S(2)}, u32[]{:S(2)}) async-start(bf16[8,512,256]{2,1,0:T(8,128)(2,1)} %bitcast.47), calls=%async_computation.2 | async-start | bytes 4194304 | tf_op jit(solution)/shard_map/all_to_all | solution.py:63
  329.9 26.2 %all-to-all-done.2 = bf16[8,512,256]{2,1,0:T(8,128)(2,1)S(1)} async-done(((bf16[8,512,256]{2,1,0:T(8,128)(2,1)}), bf16[8,512,256]{2,1,0:T(8,128)(2,1)S(1)}, u32[]{:S(2)}, u32[]{:S(2)}) %all-to-all-start.2) | async-done | bytes 2097184 | tf_op jit(solution)/shard_map/all_to_all | solution.py:63
  356.4 1.7 add_convert_fusion
  (34 shorter events, 1.4 us)
Async XLA Ops:
  6.5 14.1 %copy-start = (bf16[512,128]{1,0:T(8,128)(2,1)S(1)}, bf16[512,128]{1,0:T(8,128)(2,1)}, u32[]{:S(2)}) copy-start(bf16[512,128]{1,0:T(8,128)(2,1)} %param.12) | copy-start | bytes 393220
  6.6 155.4 %all-gather.3.cloned.1.call-start = ((), (), s32[]{:S(2)}) async-start(), calls=%async_computation.3 | async-start | bytes 6488064 | tf_op jit(solution)/shard_map/all_gather | solution.py:19
  9.3 7.3 %collective-permute-start = (bf16[2,128,128]{2,1,0:T(8,128)(2,1)S(1)}, bf16[2,128,128]{2,1,0:T(8,128)(2,1)S(1)}, u32[]{:S(2)}, u32[]{:S(2)}) collective-permute-start(bf16[2,128,128]{2,1,0:T(8,128)(2,1)S(1)} %get-tuple-element.12), channel_id=1, source_target_pairs={{0,8},{8,16},{16,24},{24,32},{32,40},{40,48},{48,56},{56,64},{64,7... | collective-permute-start | bytes 196616 | tf_op jit(solution)/shard_map/ppermute | solution.py:30
  14.6 6.1 %collective-permute-start.1 = (bf16[2,128,128]{2,1,0:T(8,128)(2,1)S(1)}, bf16[2,128,128]{2,1,0:T(8,128)(2,1)S(1)}, u32[]{:S(2)}, u32[]{:S(2)}) collective-permute-start(bf16[2,128,128]{2,1,0:T(8,128)(2,1)S(1)} %get-tuple-element.13), channel_id=1, source_target_pairs={{8,0},{16,8},{24,16},{32,24},{40,32},{48,40},{56,48},{64,56},{72,6... | collective-permute-start | bytes 196616 | tf_op jit(solution)/shard_map/ppermute | solution.py:32
  22.2 42.9 %copy-start.2 = (bf16[1024,256]{1,0:T(8,128)(2,1)S(1)}, bf16[1024,256]{1,0:T(8,128)(2,1)}, u32[]{:S(2)}) copy-start(bf16[1024,256]{1,0:T(8,128)(2,1)} %param.17) | copy-start | bytes 1572868
  23.3 56.1 %all-to-all-start = ((bf16[8,512,128]{1,2,0:T(8,128)(2,1)}), bf16[8,512,128]{1,2,0:T(8,128)(2,1)S(1)}, u32[]{:S(2)}, u32[]{:S(2)}) async-start(bf16[8,512,128]{1,2,0:T(8,128)(2,1)} %broadcast_in_dim.9), calls=%async_computation | async-start | bytes 2097152 | tf_op jit(solution)/shard_map/all_to_all | solution.py:41
  64.3 228.8 %all-gather.5.cloned.1.call-start = ((), (), s32[]{:S(2)}) async-start(), calls=%async_computation.4 | async-start | bytes 3244032 | tf_op jit(solution)/shard_map/all_gather | solution.py:76
  79.9 52.3 %copy-start.5 = (bf16[512,2048]{1,0:T(8,128)(2,1)S(1)}, bf16[512,2048]{1,0:T(8,128)(2,1)}, u32[]{:S(2)}) copy-start(bf16[512,2048]{1,0:T(8,128)(2,1)} %param.16) | copy-start | bytes 6291460
  132.2 3.0 copy-start.3
  135.8 157.3 %copy-start.1 = (bf16[512,2048]{1,0:T(8,128)(2,1)}, bf16[512,2048]{1,0:T(8,128)(2,1)S(1)}, u32[]{:S(2)}) copy-start(bf16[512,2048]{1,0:T(8,128)(2,1)S(1)} %multiply_convert_fusion) | copy-start | bytes 6291460
  135.8 33.9 %copy-start.4 = (f32[3,768]{1,0:T(4,128)S(1)}, f32[3,768]{1,0:T(4,128)}, u32[]{:S(2)}) copy-start(f32[3,768]{1,0:T(4,128)} %param.21) | copy-start | bytes 27652
  135.9 157.3 %copy-start.6 = (f32[768]{0:T(1024)S(1)}, f32[768]{0:T(1024)}, u32[]{:S(2)}) copy-start(f32[768]{0:T(1024)} %param.22) | copy-start | bytes 9220
  165.7 127.5 %collective-permute-start.2 = (bf16[1,768]{1,0:T(2,128)(2,1)S(1)}, bf16[1,768]{1,0:T(2,128)(2,1)S(1)}, u32[]{:S(2)}, u32[]{:S(2)}) collective-permute-start(bf16[1,768]{1,0:T(2,128)(2,1)S(1)} %get-tuple-element.10), channel_id=1, source_target_pairs={{0,8},{8,16},{16,24},{24,32},{32,40},{40,48},{48,56},{56,64},{64,7... | collective-permute-start | bytes 4616 | tf_op jit(solution)/shard_map/ppermute | solution.py:30
  168.4 124.7 %collective-permute-start.3 = (bf16[1,768]{1,0:T(2,128)(2,1)S(1)}, bf16[1,768]{1,0:T(2,128)(2,1)S(1)}, u32[]{:S(2)}, u32[]{:S(2)}) collective-permute-start(bf16[1,768]{1,0:T(2,128)(2,1)S(1)} %get-tuple-element.11), channel_id=1, source_target_pairs={{8,0},{16,8},{24,16},{32,24},{40,32},{48,40},{56,48},{64,56},{72,6... | collective-permute-start | bytes 4616 | tf_op jit(solution)/shard_map/ppermute | solution.py:32
  304.7 51.4 %all-to-all-start.2 = ((bf16[8,512,256]{2,1,0:T(8,128)(2,1)}), bf16[8,512,256]{2,1,0:T(8,128)(2,1)S(1)}, u32[]{:S(2)}, u32[]{:S(2)}) async-start(bf16[8,512,256]{2,1,0:T(8,128)(2,1)} %bitcast.47), calls=%async_computation.2 | async-start | bytes 4194304 | tf_op jit(solution)/shard_map/all_to_all | solution.py:63
Sparse Core Ops, SparseCore 0:
  9.4 152.4 all-gather.2
  164.0 129.0 all-gather.4
where the time goes:
time: 365 us
  waiting for transfers between devices  195 us (53%)
  starting transfers between devices  76.9 us (21%)
  blocking collectives  52.3 us (14%)
  matrix products  16.2 us (4%)
  between operations  14.3 us (4%)
  local copies, waits for them, and re-layouts  5.92 us (2%)
  other arithmetic  4.64 us (1%)
    all_gather x1, waiting for transfers between devices, shards(): whole_down = lax.all_gather(w_down, 'sp', axis=1, tiled=True)  123 us
    all_to_all x1, blocking collectives, sent_to_all(): return lax.all_to_all(copies, axis, split_axis=0, concat_axis=0, tiled=True)  52.3 us
    all_to_all x1, starting transfers between devices, sent_to_all(): return lax.all_to_all(copies, axis, split_axis=0, concat_axis=0, tiled=True)  41.1 us
    all_to_all x1, waiting for transfers between devices, sent_and_summed(): lax.all_to_all(blocks, axis, split_axis=0, concat_axis=0, tiled=True)  26.2 us
    all_gather x1, waiting for transfers between devices, sent_together(): lax.all_gather(both, axis, axis=dim, tiled=True)  26.1 us
    all_to_all x1, starting transfers between devices, sent_and_summed(): lax.all_to_all(blocks, axis, split_axis=0, concat_axis=0, tiled=True)  25.2 us
    all_to_all x1, waiting for transfers between devices, sent_to_all(): return lax.all_to_all(copies, axis, split_axis=0, concat_axis=0, tiled=True)  14.1 us
    dot_general x1, matrix products, shards(): terms = jnp.dot(act, whole_down, preferred_element_type=jnp.float32)  8.43 us
  transfers between devices with their start and end apart: 8, of which 5 were waited for; matrix products, arithmetic and copies ran while one was open for 3% of the time, Pallas kernels for 0%

commit v1 on v0

v1 whole, which is shorter than its diff:
```python
import functools

import jax
import jax.numpy as jnp
from jax import lax
from jax.experimental import pallas as pl
from jax.experimental.pallas import tpu as pltpu
from jax.sharding import PartitionSpec as P

H = 8
KVH = 2
HD = 128
WINDOW = 128
CONV = 3
EDGE = 16
MESH = pl.DeviceIdType.MESH
F32 = jnp.float32
BF16 = jnp.bfloat16


def layer_kernel(
    span,
    ranks,
    q_hbm,
    k_hbm,
    v_hbm,
    sink_ref,
    res_hbm,
    op_hbm,
    gain_ref,
    wg_hbm,
    wu_hbm,
    cw_ref,
    cb_ref,
    wd_hbm,
    out_ref,
    q_buf,
    kv_buf,
    res_buf,
    op_buf,
    mix_buf,
    summed,
    stat,
    nx_buf,
    wide,
    tall,
    accs,
    act_buf,
    theirs_out,
    theirs_in,
    hop_out,
    hop_in,
    held,
    load_sem,
    kv_send,
    kv_recv,
    z_send,
    z_recv,
    y_send,
    y_recv,
    x_send,
    x_recv,
    edge_send,
    edge_recv,
    pair_send,
    pair_recv,
    hop_send,
    hop_recv,
):
    tokens, width = res_buf.shape
    depth, hidden = wg_hbm.shape
    cols = width // ranks
    half = span // 2
    pw = wide.shape[2]
    pd = tall.shape[2]
    chips = ranks // 2

    g = lax.axis_index("grp")
    s = lax.axis_index("sp")
    t = lax.axis_index("tp")
    right, left = lax.rem(s + 1, span), lax.rem(s + span - 1, span)
    parity = lax.rem(g, 2)
    pair_grp = g + 1 - 2 * parity
    own, other = 2 * parity, 2 - 2 * parity
    core = lax.rem(t, 2)
    chip = lax.div(t, 2)
    partner = t + 1 - 2 * core
    ahead = lax.rem(t + 2 - 4 * core + ranks, ranks)
    behind = lax.rem(t - 2 + 4 * core + ranks, ranks)
    across = lax.rem(t + ranks // 2, ranks)
    kv_col = pl.multiple_of(lax.div(t * KVH, ranks) * HD, HD)

    def rows(j):
        return pl.ds(pl.multiple_of(j * depth, depth), depth)

    own_rows = rows(s)
    cut = pw - (hidden - pw)
    loads = [
        (wg_hbm.at[:, pl.ds(0, pw)], wide.at[0, own_rows, :]),
        (wg_hbm.at[:, pl.ds(pw, hidden - pw)], wide.at[1, own_rows, pl.ds(0, hidden - pw)]),
        (wu_hbm.at[:, pl.ds(0, cut)], wide.at[1, own_rows, pl.ds(hidden - pw, cut)]),
        (wu_hbm.at[:, pl.ds(cut, pw)], wide.at[2, own_rows, :]),
        (wd_hbm.at[:, pl.ds(0, pd)], tall.at[0, own_rows, :]),
        (wd_hbm.at[:, pl.ds(pd, pd)], tall.at[1, own_rows, :]),
        (wd_hbm.at[:, pl.ds(2 * pd, pd)], tall.at[2, own_rows, :]),
        (k_hbm.at[:, pl.ds(kv_col, HD)], kv_buf.at[0, pl.ds(WINDOW, tokens), :]),
        (v_hbm.at[:, pl.ds(kv_col, HD)], kv_buf.at[1, pl.ds(WINDOW, tokens), :]),
        (q_hbm, q_buf),
        (op_hbm, op_buf.at[t]),
        (res_hbm, res_buf),
    ]
    loads = [pltpu.make_async_copy(a, b, load_sem.at[i]) for i, (a, b) in enumerate(loads)]

    barrier = pltpu.get_barrier_semaphore()
    greeted = ({"sp": right}, {"sp": left}, {"grp": pair_grp}, {"tp": ahead}, {"tp": behind}, {"tp": partner})
    for who in greeted:
        pl.semaphore_signal(barrier, inc=1, device_id=who, device_id_type=MESH)
    for copy in loads:
        copy.start()

    def remote(src, dst, send, recv, who):
        return pltpu.make_async_remote_copy(
            src_ref=src, dst_ref=dst, send_sem=send, recv_sem=recv, device_id=who, device_id_type=MESH
        )

    def part(kind, index, j):
        return (wide if kind == 0 else tall).at[index, rows(j), :]

    def z_copy(kind, ab, j, way):
        ref = part(kind, own if ab else 1, j)
        row = 2 * kind + ab
        return remote(ref, ref, z_send.at[way, row], z_recv.at[row, j], {"sp": left if way else right})

    def y_copy(kind, j):
        ref = part(kind, own, j)
        return remote(ref, ref, y_send.at[kind], y_recv.at[kind, j], {"grp": pair_grp})

    def y_arrived(kind, j):
        ref = part(kind, other, j)
        remote(ref, ref, y_send.at[kind], y_recv.at[kind, j], {"grp": pair_grp}).wait_recv()

    def block(kind, b):
        if kind == 0:
            return op_buf.at[b]
        return mix_buf.at[:, pl.ds(pl.multiple_of(b * HD, HD), HD)]

    def x_copy(kind, b, slot, who):
        ref = block(kind, b)
        return remote(ref, ref, x_send.at[kind, slot], x_recv.at[kind, b], {"tp": who})

    def x_open(kind):
        x_copy(kind, t, 0, ahead).start()
        x_copy(kind, t, 1, behind).start()
        x_copy(kind, t, 2, partner).start()

    def x_pass(kind):
        x_copy(kind, behind, 3, ahead).wait_recv()
        x_copy(kind, behind, 3, ahead).start()
        x_copy(kind, behind, 4, partner).start()
        x_copy(kind, ahead, 5, partner).wait_recv()
        x_copy(kind, ahead, 5, partner).start()

    def x_last(kind):
        x_copy(kind, across, 6, partner).wait_recv()
        x_copy(kind, across, 6, partner).start()

    def x_close(kind):
        for step in range(chips):
            b = lax.rem(partner + 2 * step, ranks)
            x_copy(kind, b, 0, partner).wait_recv()

    def kv_copy(way):
        if way == 0:
            src, dst = kv_buf.at[:, pl.ds(tokens, WINDOW), :], kv_buf.at[:, pl.ds(0, WINDOW), :]
        else:
            src, dst = kv_buf.at[:, pl.ds(WINDOW, WINDOW), :], kv_buf.at[:, pl.ds(WINDOW + tokens, WINDOW), :]
        return remote(src, dst, kv_send.at[way], kv_recv.at[way], {"sp": left if way else right})

    def edge_copy(way):
        if way == 0:
            src, dst = nx_buf.at[pl.ds(tokens, EDGE), :], nx_buf.at[pl.ds(0, EDGE), :]
        else:
            src, dst = nx_buf.at[pl.ds(EDGE, EDGE), :], nx_buf.at[pl.ds(EDGE + tokens, EDGE), :]
        return remote(src, dst, edge_send.at[way], edge_recv.at[way], {"sp": left if way else right})

    def attend(i):
        lo = i * WINDOW
        keys = kv_buf[0, lo : lo + 3 * WINDOW, :]
        vals = kv_buf[1, lo : lo + 3 * WINDOW, :]
        scores = lax.dot_general(
            q_buf[lo : lo + WINDOW, :], keys, (((1,), (1,)), ((), ())), preferred_element_type=F32
        ) * (HD ** (-0.5))
        row = lax.broadcasted_iota(jnp.int32, scores.shape, 0)
        col = lax.broadcasted_iota(jnp.int32, scores.shape, 1)
        pos = s * tokens + (lo - WINDOW) + col
        gap = col - row
        seen = (gap >= 0) & (gap <= 2 * WINDOW) & (pos >= 0) & (pos < span * tokens)
        scores = jnp.where(seen, scores, F32(-1e30))
        sink = sink_ref[0]
        top = jnp.maximum(jnp.max(scores, axis=-1, keepdims=True), sink)
        expo = jnp.exp(scores - top)
        total = jnp.sum(expo, axis=-1, keepdims=True) + jnp.exp(sink - top)
        weights = (expo / total).astype(BF16)
        mixed = jnp.dot(weights, vals, preferred_element_type=F32).astype(BF16)
        mix_buf[lo : lo + WINDOW, pl.ds(pl.multiple_of(t * HD, HD), HD)] = mixed

    def project(o):
        at = slice(o * cols, (o + 1) * cols)
        block_sum = res_buf[:, at].astype(F32) + jnp.dot(mix_buf[...], op_buf[o], preferred_element_type=F32)
        summed[:, at] = block_sum
        first, second = block_sum[:, : cols // 2], block_sum[:, cols // 2 :]
        lone = first + second
        squares = first * first + second * second
        if o == 0:
            stat[0] = lone
            stat[1] = squares
        else:
            stat[0] += lone
            stat[1] += squares

    def normalize(lo, hi):
        @pl.loop(lo // EDGE, hi // EDGE)
        def _(i):
            at = pl.ds(pl.multiple_of(i * EDGE, EDGE), EDGE)
            mean = jnp.sum(stat[0, at, :], axis=-1, keepdims=True) / width
            msq = jnp.sum(stat[1, at, :], axis=-1, keepdims=True) / width
            scale = lax.rsqrt(msq - mean * mean + 1e-05)
            normed = (summed[at, :] - mean) * scale * gain_ref[...]
            nx_buf[pl.ds(pl.multiple_of(i * EDGE + EDGE, EDGE), EDGE), :] = normed.astype(BF16)

    quads = span * depth // cols
    mine = lax.div(s * depth, cols)

    def gates(shift, first=False):
        quad = lax.rem(mine + shift + quads, quads)
        for i in range(cols // depth):
            j = quad * (cols // depth) + i

            @pl.when(j != s)
            def _():
                y_arrived(0, j)

        at = pl.ds(pl.multiple_of(quad * cols, cols), cols)
        x = nx_buf[:, at]
        for p in range(3):
            y = jnp.dot(x, wide[p, at, :], preferred_element_type=F32)
            if first:
                accs[p] = y
            else:
                accs[p] += y

    def edge_zero(where):
        for p in range(2):
            accs[p, where : where + EDGE, :] = jnp.zeros((EDGE, pw), F32)

    def activate():
        for h in range(3):
            gp, gc = divmod(h * pd, pw)
            up, uc = divmod(hidden + h * pd, pw)
            for r in range(0, tokens, WINDOW):
                conv = cb_ref[h * pd : (h + 1) * pd].reshape(1, pd)
                for tap in range(CONV):
                    lo = EDGE - CONV // 2 + tap + r
                    gate = accs[gp, lo : lo + WINDOW, gc : gc + pd].astype(BF16).astype(F32)
                    conv = conv + gate * cw_ref[tap : tap + 1, h * pd : (h + 1) * pd]
                ups = accs[up, EDGE + r : EDGE + r + WINDOW, uc : uc + pd].astype(BF16).astype(F32)
                act = conv / (1.0 + jnp.exp(-conv)) * ups
                act_buf[r : r + WINDOW, h * pd : (h + 1) * pd] = act.astype(BF16)

    def partial(o):
        at = pl.ds(pl.multiple_of(o * cols, cols), cols)
        total = None
        for p in range(3):
            term = lax.dot_general(
                act_buf[:, p * pd : (p + 1) * pd],
                tall[p, at, :],
                (((1,), (1,)), ((), ())),
                preferred_element_type=F32,
            )
            total = term if total is None else total + term
        return total

    def pair_copy(owner):
        return remote(
            theirs_out.at[owner], theirs_in.at[owner], pair_send.at[owner], pair_recv.at[owner], {"tp": partner}
        )

    def hop_copy(i):
        return remote(hop_out.at[i], hop_in.at[i], hop_send.at[i], hop_recv.at[i], {"tp": behind if i == 1 else ahead})

    def give(owner):
        theirs_out[owner] = partial(2 * owner + 1 - core).astype(BF16)

    def joined(owner):
        kept = partial(2 * owner + core)
        pair_copy(owner).wait_recv()
        return kept + theirs_in[owner].astype(F32)

    for i in range(9):
        loads[i].wait()
    pl.semaphore_wait(barrier, len(greeted))
    for way in range(2):
        kv_copy(way).start()
    for kind in range(2):
        for ab in range(2):
            for way in range(2):
                z_copy(kind, ab, s, way).start()
    loads[10].wait()
    x_open(0)
    loads[9].wait()

    def unit_attend(blocks, last):
        if not last:
            for way in range(2):
                kv_copy(way).wait_recv()
        for i in blocks:
            attend(i)
        if last:
            x_open(1)

    def unit_last():
        x_last(0)
        x_last(1)

    def unit_project(blocks):
        if blocks[0] == 0:
            x_close(0)
            x_close(1)
            loads[11].wait()
        for o in blocks:
            project(o)

    def unit_normalize(lo, hi):
        normalize(lo, hi)
        if hi == tokens:
            for way in range(2):
                edge_copy(way).start()

    def unit_gates(shifts, first=False):
        if first:
            for way in range(2):
                edge_copy(way).wait_recv()
        for i, shift in enumerate(shifts):
            gates(shift, first and i == 0)

    blocks = tokens // WINDOW
    units = {
        (1, 0): lambda: unit_attend(range(blocks // 2), False),
        (1, 1): lambda: unit_attend(range(blocks // 2, blocks), True),
        (3, 1): lambda: x_pass(0),
        (4, 0): lambda: x_pass(1),
        (5, 1): unit_last,
        (6, 0): lambda: unit_project([0, 1]),
        (6, 1): lambda: unit_project([2, 3]),
        (7, 0): lambda: unit_project([4, 5]),
        (7, 1): lambda: unit_project([6, 7]),
        (8, 0): lambda: unit_normalize(0, tokens // 2),
        (8, 1): lambda: unit_normalize(tokens // 2, tokens),
        (9, 1): lambda: unit_gates([0], True),
        (10, 0): lambda: unit_gates([1]),
        (10, 1): lambda: unit_gates([-1]),
        (12, 0): lambda: unit_gates([2]),
        (12, 1): lambda: unit_gates([-2]),
    }

    @pl.loop(1, half)
    def _(k):
        back = lax.rem(s - k + span, span)
        front = lax.rem(s + k, span)
        for kind in range(2):
            for ab in range(2):
                for way, j in ((0, back), (1, front)):
                    z_copy(kind, ab, j, way).wait_recv()
                    if ab == way:
                        z_copy(kind, ab, j, way).start()
                    else:

                        @pl.when(k < half - 1)
                        def _():
                            z_copy(kind, ab, j, way).start()

                    if ab == 1:
                        y_copy(kind, j).start()
            for (step, slot), unit in units.items():
                if slot == kind:
                    pl.when(k == step)(unit)

    far = lax.rem(s + half, span)
    for kind in range(2):
        z_copy(kind, 0, far, 0).wait_recv()
        z_copy(kind, 1, far, 1).wait_recv()
        y_copy(kind, far).start()

    gates(3)
    gates(-3)
    gates(4)

    @pl.when(s == 0)
    def _():
        edge_zero(0)

    @pl.when(s == span - 1)
    def _():
        edge_zero(EDGE + tokens)

    activate()

    @pl.loop(1, span)
    def _(k):
        y_arrived(1, lax.rem(s + k, span))

    chip_across = lax.div(across, 2)
    chip_ahead = lax.div(ahead, 2)
    chip_behind = lax.div(behind, 2)
    give(chip_across)
    give(chip_behind)
    pair_copy(chip_across).start()
    give(chip_ahead)
    pair_copy(chip_behind).start()
    pair_copy(chip_ahead).start()
    hop_out[0] = joined(chip_across).astype(BF16)
    hop_copy(0).start()
    hop_out[1] = joined(chip_behind).astype(BF16)
    give(chip)
    hop_copy(1).start()
    pair_copy(chip).start()
    held[0] = joined(chip_ahead)
    own_cols = pl.ds(pl.multiple_of(t * cols, cols), cols)
    held[1] = joined(chip) + nx_buf[EDGE : EDGE + tokens, own_cols].astype(F32)
    hop_copy(0).wait_recv()
    hop_out[2] = (held[0] + hop_in[0].astype(F32)).astype(BF16)
    hop_copy(2).start()
    hop_copy(1).wait_recv()
    held[1] += hop_in[1].astype(F32)
    hop_copy(2).wait_recv()
    out_ref[...] = (held[1] + hop_in[2].astype(F32)).astype(BF16)

    for way in range(2):
        kv_copy(way).wait_send()
        edge_copy(way).wait_send()
        for kind in range(2):
            for ab in range(2):
                n = half if ab == way else half - 1
                ref = (wide if kind == 0 else tall).at[0, pl.ds(0, n * depth), :]
                row = 2 * kind + ab
                remote(ref, ref, z_send.at[way, row], z_recv.at[row, 0], {"sp": right}).wait_send()
    for kind in range(2):
        ref = (wide if kind == 0 else tall).at[0, pl.ds(0, (span - 1) * depth), :]
        remote(ref, ref, y_send.at[kind], y_recv.at[kind, 0], {"grp": pair_grp}).wait_send()
        for slot in range(7):
            x_copy(kind, t, slot, partner).wait_send()
    for owner in range(chips):
        pair_copy(owner).wait_send()
    for i in range(3):
        hop_copy(i).wait_send()


def solution(mesh):
    span, ranks = mesh.shape["sp"], mesh.shape["tp"]

    def shards(q, k, v, sink, resid, out_proj, gain, w_gate, w_up, conv_w, conv_b, w_down):
        tokens, width = resid.shape
        depth, hidden = w_gate.shape
        cols = width // ranks
        chips = ranks // 2
        pw, pd = 2 * hidden // 3, hidden // 3
        whole = pl.BlockSpec(memory_space=pltpu.VMEM)
        there = pl.BlockSpec(memory_space=pl.ANY)
        scalar = pl.BlockSpec(memory_space=pltpu.SMEM)
        dma = pltpu.SemaphoreType.DMA
        return pl.pallas_call(
            functools.partial(layer_kernel, span, ranks),
            out_shape=jax.ShapeDtypeStruct((tokens, cols), BF16),
            in_specs=[there, there, there, scalar, there, there, whole, there, there, whole, whole, there],
            out_specs=whole,
            scratch_shapes=[
                pltpu.VMEM((tokens, HD), BF16),
                pltpu.VMEM((2, tokens + 2 * WINDOW, HD), BF16),
                pltpu.VMEM((tokens, width), BF16),
                pltpu.VMEM((ranks, out_proj.shape[0], cols), BF16),
                pltpu.VMEM((tokens, ranks * HD), BF16),
                pltpu.VMEM((tokens, width), F32),
                pltpu.VMEM((2, tokens, cols // 2), F32),
                pltpu.VMEM((tokens + 2 * EDGE, width), BF16),
                pltpu.VMEM((3, span * depth, pw), BF16),
                pltpu.VMEM((3, span * depth, pd), BF16),
                pltpu.VMEM((3, tokens + 2 * EDGE, pw), F32),
                pltpu.VMEM((tokens, hidden), BF16),
                pltpu.VMEM((chips, tokens, cols), BF16),
                pltpu.VMEM((chips, tokens, cols), BF16),
                pltpu.VMEM((3, tokens, cols), BF16),
                pltpu.VMEM((3, tokens, cols), BF16),
                pltpu.VMEM((2, tokens, cols), F32),
                dma((12,)),
                dma((2,)),
                dma((2,)),
                dma((2, 4)),
                dma((4, span)),
                dma((2,)),
                dma((2, span)),
                dma((2, 7)),
                dma((2, ranks)),
                dma((2,)),
                dma((2,)),
                dma((chips,)),
                dma((chips,)),
                dma((3,)),
                dma((3,)),
            ],
            compiler_params=pltpu.CompilerParams(
                collective_id=0, has_side_effects=True, vmem_limit_bytes=60 * 1024 * 1024
            ),
        )(
            q, k, v, sink, resid, out_proj, gain.reshape(1, width), w_gate, w_up,
            conv_w, conv_b, w_down.T,
        )

    return jax.shard_map(
        shards,
        mesh=mesh,
        in_specs=(
            P(("grp", "sp"), "tp"),
            P(("grp", "sp"), None),
            P(("grp", "sp"), None),
            P("tp"),
            P(("grp", "sp"), None),
            P(None, "tp"),
            P(),
            P("sp", "tp"),
            P("sp", "tp"),
            P(None, "tp"),
            P("tp"),
            P("tp", "sp"),
        ),
        out_specs=P(("grp", "sp"), "tp"),
        check_vma=False,
    )
```

time: 365 us -> 145 us (0.40)
  waiting for transfers between devices: 195 us -> 0 us
  Pallas kernels: 0 us -> 141 us
  starting transfers between devices: 76.9 us -> 0 us
  blocking collectives: 52.3 us -> 0 us
  matrix products: 16.2 us -> 0 us
  between operations: 14.3 us -> 0.66 us
  other arithmetic: 4.64 us -> 0 us
  local copies, waits for them, and re-layouts: 5.92 us -> 1.67 us
    all_gather x2 -> x0, waiting for transfers between devices: 149 us -> none  [the longest x1 123 us: shards(): whole_down = lax.all_gather(w_down, 'sp', axis=1, tiled=True)]
    pallas_call x0 -> x1, Pallas kernels: none -> 141 us  [shards(): pl.pallas_call(functools.partial(layer_kernel, span, ranks), out_shape=ja...]
    all_to_all x2 -> x0, starting transfers between devices: 66.3 us -> none  [the longest x1 41.1 us: sent_to_all(): return lax.all_to_all(copies, axis, split_axis=0, concat_axis=0, tiled=True)]
    all_to_all x1 -> x0, blocking collectives: 52.3 us -> none  [sent_to_all(): return lax.all_to_all(copies, axis, split_axis=0, concat_axis=0, tiled=True)]
    all_to_all x2 -> x0, waiting for transfers between devices: 40.3 us -> none  [the longest x1 26.2 us: sent_and_summed(): lax.all_to_all(blocks, axis, split_axis=0, concat_axis=0, tiled=True)]
    dot_general x5 -> x0, matrix products: 16.2 us -> none  [the longest x1 8.43 us: shards(): terms = jnp.dot(act, whole_down, preferred_element_type=jnp.float32)]
    ppermute x4 -> x0, starting transfers between devices: 10.6 us -> none  [the longest x2 8.03 us: with_halo(): lax.ppermute(tail, axis, [(i, (i + 1) % count) for i in range(ends)])]
    ppermute x4 -> x0, waiting for transfers between devices: 4.07 us -> none  [the longest x2 4.07 us: with_halo(): lax.ppermute(head, axis, [((i + 1) % count, i) for i in range(ends)])]
  transfers between devices with their start and end apart: 8 -> 0, of which waited for: 5 -> 0; matrix products, arithmetic and copies ran while one was open for 3% -> 0% of each run, Pallas kernels for 0% -> 0%
where the time goes in v1:
time: 145 us; the launch traced here: 144 us
  Pallas kernels  141 us (97%)
  local copies, waits for them, and re-layouts  1.67 us (1%)
    pallas_call x1, Pallas kernels, shards(): pl.pallas_call(functools.partial(layer_kernel, span, ranks), out_shape=ja...  141 us

profile of v1, /device:TPU:33, one launch (start us, length us, event | category | flops | bytes accessed | tf_op | source)
XLA Modules:
  0.0 143.8 jit_solution(3372470027146881322)
XLA Ops:
  0.7 141.5 %shard_map.118 = bf16[512,256]{1,0:T(8,128)(2,1)} custom-call(bf16[512,128]{1,0:T(8,128)(2,1)} %q_hbm.1, bf16[512,256]{1,0:T(8,128)(2,1)} %k_hbm.1, bf16[512,256]{1,0:T(8,128)(2,1)} %v_hbm.1, f32[1]{0:T(128)S(6)} %copy.14.sink_ref, bf16[512,2048]{1,0:T(8,128)(2,1)} %res_hbm.1, bf16[1024,256]{1,0:T(8,128)(2,1)} %op_hbm.1, f32[1,2048]{1,0:T(1,128)} %bitcast.3, ...), custom_call_target="tpu_custom_call" | custom-call | tf_op jit(solution)/shard_map/pallas_call | solution.py:471
  142.2 1.7 %copy.15 = bf16[512,256]{1,0:T(8,128)(2,1)} copy(bf16[512,256]{1,0:T(8,128)(2,1)} %shard_map.118) | data formatting | bytes 524288
